TPU v7x, 32 devices: a whole 2x2x4 slice. The times are simulated.
32 devices in a mesh: rep: 2 (over x), fs: 4 (over z), tp: 4 (over y, core).
Axes of the slice: x: 2, y: 2, z: 4, core: 2. Of those that a mesh axis runs over, the one named last changes fastest.
Arguments:
- tokens: bfloat16 [8192, 2048], P(('rep', 'fs'), 'tp'), may hold values from -6 to 6
- mix_in_gain: bfloat16 [2048], replicated, may hold values from 0.099609375 to 1.8984375
- bgate_weight: bfloat16 [2048, 2048], P('fs', 'tp'), may hold values from -0.125 to 0.125
- cgate_weight: bfloat16 [2048, 2048], P('fs', 'tp'), may hold values from -0.125 to 0.125
- value_weight: bfloat16 [2048, 2048], P('fs', 'tp'), may hold values from -0.125 to 0.125
- conv_taps: bfloat16 [3, 2048], replicated, may hold values from -3 to 3
- out_weight: bfloat16 [2048, 2048], P('tp', 'fs'), may hold values from -0.41984465 to 0.41984465
- mix_out_gain: bfloat16 [2048], replicated, may hold values from 0.099609375 to 1.8984375
- ffn_in_gain: bfloat16 [2048], replicated, may hold values from 0.099609375 to 1.8984375
- up_weight: bfloat16 [2048, 8192], P('fs', 'tp'), may hold values from -0.125 to 0.125
- down_weight: bfloat16 [8192, 2048], P('tp', 'fs'), may hold values from -0.20992233 to 0.20992233
- ffn_out_gain: bfloat16 [2048], replicated, may hold values from 0.099609375 to 1.8984375
Outputs:
- result: bfloat16 [8192, 2048], P(('rep', 'fs'), 'tp')
All inputs are finite; a program needn't handle non-finite values.
Results may differ from a plain program's by a relative error of at most 0.02.
Values may be sent and summed in bfloat16 or wider, within the bound.
A program may use at most 128 MiB of HBM per device.

v0:
```python
import jax
import jax.numpy as jnp
from jax import lax
from jax.sharding import PartitionSpec as P

LEN = 256
epsilon = 1e-06


def normalize(rows, gain):
    rows = rows.astype(jnp.float32)
    factor = lax.rsqrt(jnp.mean(rows * rows, axis=-1, keepdims=True) + epsilon)
    return rows * factor * gain.astype(jnp.float32)


def convolve(inner, taps):
    seqs = inner.reshape(-1, LEN, inner.shape[1])
    padded = jnp.pad(seqs, ((0, 0), (1, 1), (0, 0)))
    weights = taps.astype(jnp.float32)
    out = weights[0] * padded[:, :-2] + weights[1] * padded[:, 1:-1] + weights[2] * padded[:, 2:]
    return out.reshape(inner.shape)


def body(
    tokens,
    mix_in_gain,
    bgate_weight,
    cgate_weight,
    value_weight,
    conv_taps,
    out_weight,
    mix_out_gain,
    ffn_in_gain,
    up_weight,
    down_weight,
    ffn_out_gain,
):
    column = lax.axis_index("tp")
    own_width = tokens.shape[1]
    first = column * own_width
    full_width = mix_in_gain.shape[0]
    whole = lax.all_gather(tokens, "tp", axis=1, tiled=True)
    normed = normalize(whole, mix_in_gain).astype(jnp.bfloat16)

    def add_rows(piece):
        return jnp.dot(normed, piece, preferred_element_type=jnp.float32)

    bgate = add_rows(lax.all_gather(bgate_weight, "fs", axis=0, tiled=True))
    cgate = add_rows(lax.all_gather(cgate_weight, "fs", axis=0, tiled=True))
    value = add_rows(lax.all_gather(value_weight, "fs", axis=0, tiled=True))
    bgate = bgate.astype(jnp.bfloat16)
    cgate = cgate.astype(jnp.bfloat16)
    value = value.astype(jnp.bfloat16)
    channels = bgate.shape[1]
    own_taps = lax.dynamic_slice_in_dim(conv_taps, column * channels, channels, 1)
    inner = cgate.astype(jnp.float32) * value.astype(jnp.float32)
    gated = (bgate.astype(jnp.float32) * convolve(inner, own_taps)).astype(jnp.bfloat16)
    partial_mix = jnp.dot(
        gated,
        lax.all_gather(out_weight, "fs", axis=1, tiled=True),
        preferred_element_type=jnp.float32,
    )
    mixed = lax.psum(partial_mix.astype(jnp.bfloat16), "tp").astype(jnp.float32)
    resid = (whole.astype(jnp.float32) + normalize(mixed, mix_out_gain)).astype(jnp.bfloat16)
    resid_own = lax.dynamic_slice_in_dim(resid, first, own_width, 1)
    second = normalize(resid, ffn_in_gain).astype(jnp.bfloat16)
    lifted = jnp.dot(
        second,
        lax.all_gather(up_weight, "fs", axis=0, tiled=True),
        preferred_element_type=jnp.float32,
    )
    active = jnp.square(jnp.maximum(lifted, 0.0)).astype(jnp.bfloat16)
    partial_ffn = jnp.dot(
        active,
        lax.all_gather(down_weight, "fs", axis=1, tiled=True),
        preferred_element_type=jnp.float32,
    )
    ffn = lax.psum_scatter(
        partial_ffn.astype(jnp.bfloat16), "tp", scatter_dimension=1, tiled=True
    ).astype(jnp.float32)
    ffn_energy = lax.psum(jnp.sum(ffn * ffn, axis=1), "tp")
    out_gain = lax.dynamic_slice_in_dim(ffn_out_gain, first, own_width, 0).astype(jnp.float32)
    closing = ffn * lax.rsqrt(ffn_energy[:, None] / full_width + epsilon) * out_gain
    return (resid_own.astype(jnp.float32) + closing).astype(jnp.bfloat16)


def solution(mesh):
    placed = (
        P(("rep", "fs"), "tp"),
        P(),
        P("fs", "tp"),
        P("fs", "tp"),
        P("fs", "tp"),
        P(),
        P("tp", "fs"),
        P(),
        P(),
        P("fs", "tp"),
        P("tp", "fs"),
        P(),
    )
    return jax.shard_map(
        body, mesh=mesh, in_specs=placed, out_specs=P(("rep", "fs"), "tp"), check_vma=False
    )
```

profile of v0, /device:TPU:0, one launch (start us, length us, event | category | flops | bytes accessed | tf_op | source)
XLA Modules:
  0.0 707.6 jit_solution(8818610116150277627)
XLA Ops:
  6.5 0.0 all-gather.8.cloned.1.call-start
  6.5 0.7 all-gather.8.cloned.1.call-update
  7.3 0.0 all-gather.12.cloned.1.call-start
  7.3 0.7 all-gather.12.cloned.1.call-update
  8.0 0.0 all-gather.14.cloned.1.call-start
  8.1 0.7 all-gather.14.cloned.1.call-update
  8.7 0.0 all-gather.10.cloned.1.call-start
  8.8 0.5 all-gather.10.cloned.1.call-update
  9.3 0.0 all-gather.16.cloned.1.call-start
  9.4 0.5 all-gather.16.cloned.1.call-update
  9.9 0.0 all-reduce.3.cloned.1.call-start
  10.0 0.7 dynamic-slice_convert_fusion
  10.7 0.7 convert_element_type.76
  11.4 34.8 %all-gather.8.cloned.1.call-done = bf16[1024,2048]{1,0:T(8,128)(2,1)} async-done(((bf16[1024,512]{1,0:T(8,128)(2,1)}), bf16[1024,2048]{1,0:T(8,128)(2,1)}) %all-gather.8.cloned.1.call-update) | async-done | bytes 4194320 | tf_op jit(solution)/shard_map/all_gather | solution.py:42
  46.1 3.1 fusion.5
  49.2 44.2 %all-gather.12.cloned.1.call-done = bf16[2048,512]{1,0:T(8,128)(2,1)} async-done(((bf16[512,512]{1,0:T(8,128)(2,1)}), bf16[2048,512]{1,0:T(8,128)(2,1)}) %all-gather.12.cloned.1.call-update) | async-done | bytes 2097168 | tf_op jit(solution)/shard_map/all_gather | solution.py:49
  93.4 5.2 convolution_convert_fusion.2
  98.6 40.8 %all-gather.14.cloned.1.call-done = bf16[2048,512]{1,0:T(8,128)(2,1)} async-done(((bf16[512,512]{1,0:T(8,128)(2,1)}), bf16[2048,512]{1,0:T(8,128)(2,1)}) %all-gather.14.cloned.1.call-update) | async-done | bytes 2097168 | tf_op jit(solution)/shard_map/all_gather | solution.py:50
  139.4 5.2 convert_multiply_fusion.8
  144.7 0.6 multiply_add_fusion
  145.3 40.0 %all-gather.10.cloned.1.call-done = bf16[2048,512]{1,0:T(8,128)(2,1)} async-done(((bf16[512,512]{1,0:T(8,128)(2,1)}), bf16[2048,512]{1,0:T(8,128)(2,1)}) %all-gather.10.cloned.1.call-update) | async-done | bytes 2097168 | tf_op jit(solution)/shard_map/all_gather | solution.py:48
  185.4 5.2 fusion.25
  190.6 40.7 %all-gather.16.cloned.1.call-done = bf16[512,2048]{1,0:T(8,128)(2,1)} async-done(((bf16[512,512]{1,0:T(8,128)(2,1)}), bf16[512,2048]{1,0:T(8,128)(2,1)}) %all-gather.16.cloned.1.call-update) | async-done | bytes 2097168 | tf_op jit(solution)/shard_map/all_gather | solution.py:60
  231.3 5.9 convolution_convert_fusion
  237.2 0.0 copy-start.1
  237.2 0.0 copy-start.2
  237.2 0.0 all-reduce.3.cloned.1.call-update
  237.2 0.0 all-gather.18.cloned.1.call-start
  237.2 0.7 all-gather.18.cloned.1.call-update
  237.9 0.0 all-gather.20.cloned.1.call-start
  238.0 0.7 all-gather.20.cloned.1.call-update
  238.7 0.2 reduce-scatter.2.cloned.1.call-start
  238.9 0.0 copy-done.1
  238.9 0.0 copy-done.2
  239.0 82.7 %all-reduce.3.cloned.1.call-done = bf16[1024,2048]{1,0:T(8,128)(2,1)} async-done(((bf16[1024,2048]{1,0:T(8,128)(2,1)}), bf16[1024,2048]{1,0:T(8,128)(2,1)}) %all-reduce.3.cloned.1.call-update) | async-done | bytes 4194320 | tf_op jit(solution)/shard_map/psum | solution.py:63
  321.6 0.0 copy-start
  321.6 3.2 fusion
  324.9 0.2 copy-done
  325.1 5.3 fusion.2
  330.4 142.6 %all-gather.18.cloned.1.call-done = bf16[2048,2048]{1,0:T(8,128)(2,1)} async-done(((bf16[512,2048]{1,0:T(8,128)(2,1)}), bf16[2048,2048]{1,0:T(8,128)(2,1)}) %all-gather.18.cloned.1.call-update) | async-done | bytes 8388624 | tf_op jit(solution)/shard_map/all_gather | solution.py:69
  473.0 149.4 %all-gather.20.cloned.1.call-done = bf16[2048,2048]{1,0:T(8,128)(2,1)} async-done(((bf16[2048,512]{1,0:T(8,128)(2,1)}), bf16[2048,2048]{1,0:T(8,128)(2,1)}) %all-gather.20.cloned.1.call-update) | async-done | bytes 8388624 | tf_op jit(solution)/shard_map/all_gather | solution.py:75
  622.4 25.7 %fusion.18 = bf16[1024,2048]{1,0:T(8,128)(2,1)} fusion(bf16[2048,2048]{1,0:T(8,128)(2,1)} %all-gather.20.cloned.1.call-done, bf16[2048,2048]{1,0:T(8,128)(2,1)} %all-gather.18.cloned.1.call-done, bf16[1024,2048]{1,0:T(8,128)(2,1)} %get-tuple-element.6, f32[2048]{0:T(1024)S(1)} %convert_element_type.92, f32[1024]{0:T(1024)S(1)} %add_rsqrt_fusion.1), kind=kOutput, calls=%fused_computation.22 | convolution fusion | flops 17196646400 | bytes 25178112 | tf_op jit(solution)/shard_map/dot_general | solution.py:73
  648.1 0.0 reduce-scatter.2.cloned.1.call-update
  648.1 0.8 dynamic-slice_convert_fusion.1
  648.8 41.9 %reduce-scatter.2.cloned.1.call-done = bf16[1024,512]{1,0:T(8,128)(2,1)} async-done(((bf16[1024,2048]{1,0:T(8,128)(2,1)}), bf16[1024,512]{1,0:T(8,128)(2,1)}) %reduce-scatter.2.cloned.1.call-update) | async-done | bytes 1048592 | tf_op jit(solution)/shard_map/reduce_scatter | solution.py:78
  690.8 1.5 fusion.21
  692.3 5.8 psum.15
  698.1 3.0 fusion.24
  (7 shorter events, 0.0 us)
Async XLA Ops:
  6.5 39.6 %all-gather.8.cloned.1.call-start = ((), (), s32[]{:S(2)}) async-start(), calls=%async_computation.1 | async-start | bytes 5242880 | tf_op jit(solution)/shard_map/all_gather | solution.py:42
  7.3 86.1 %all-gather.12.cloned.1.call-start = ((), (), s32[]{:S(2)}) async-start(), calls=%async_computation.3 | async-start | bytes 2621440 | tf_op jit(solution)/shard_map/all_gather | solution.py:49
  8.0 131.4 %all-gather.14.cloned.1.call-start = ((), (), s32[]{:S(2)}) async-start(), calls=%async_computation.4 | async-start | bytes 2621440 | tf_op jit(solution)/shard_map/all_gather | solution.py:50
  8.7 176.6 %all-gather.10.cloned.1.call-start = ((), (), s32[]{:S(2)}) async-start(), calls=%async_computation.2 | async-start | bytes 2621440 | tf_op jit(solution)/shard_map/all_gather | solution.py:48
  9.3 221.9 %all-gather.16.cloned.1.call-start = ((), (), s32[]{:S(2)}) async-start(), calls=%async_computation.5 | async-start | bytes 2621440 | tf_op jit(solution)/shard_map/all_gather | solution.py:60
  9.9 311.7 %all-reduce.3.cloned.1.call-start = ((), (), s32[]{:S(2)}) async-start(), calls=%async_computation.6 | async-start | bytes 8388608 | tf_op jit(solution)/shard_map/psum | solution.py:63
  237.2 1.8 copy-start.1
  237.2 1.8 copy-start.2
  237.2 235.8 %all-gather.18.cloned.1.call-start = ((), (), s32[]{:S(2)}) async-start(), calls=%async_computation.7 | async-start | bytes 10485760 | tf_op jit(solution)/shard_map/all_gather | solution.py:69
  237.9 384.4 %all-gather.20.cloned.1.call-start = ((), (), s32[]{:S(2)}) async-start(), calls=%async_computation.8 | async-start | bytes 10485760 | tf_op jit(solution)/shard_map/all_gather | solution.py:75
  238.7 452.1 %reduce-scatter.2.cloned.1.call-start = ((), (), s32[]{:S(2)}) async-start(), calls=%async_computation.9 | async-start | bytes 5242880 | tf_op jit(solution)/shard_map/reduce_scatter | solution.py:78
  321.6 3.4 copy-start
Sparse Core Ops, SparseCore 0:
  8.9 37.1 all-gather.7
  47.7 45.6 all-gather.11
  94.9 44.4 all-gather.13
  140.9 44.4 all-gather.9
  186.8 44.4 all-gather.15
  237.3 84.2 all-reduce.2
  323.2 149.7 all-gather.17
  474.6 147.7 all-gather.19
  648.2 42.5 reduce-scatter.1
where the time goes:
time: 708 us
  waiting for transfers between devices  622 us (88%)
  matrix products  47.3 us (7%)
  other arithmetic  18.9 us (3%)
  between operations  13.3 us (2%)
    all_gather x1, waiting for transfers between devices, body(): lax.all_gather(down_weight, 'fs', axis=1, tiled=True)  149 us
    all_gather x1, waiting for transfers between devices, body(): lax.all_gather(up_weight, 'fs', axis=0, tiled=True)  143 us
    psum x1, waiting for transfers between devices, body(): mixed = lax.psum(partial_mix.astype(jnp.bfloat16), 'tp').astype(jnp.float32)  82.7 us
    all_gather x1, waiting for transfers between devices, body(): cgate = add_rows(lax.all_gather(cgate_weight, 'fs', axis=0, tiled=True))  44.2 us
    reduce_scatter x1, waiting for transfers between devices, body(): lax.psum_scatter(partial_ffn.astype(jnp.bfloat16), 'tp', scatter_dimensio...  41.9 us
    all_gather x1, waiting for transfers between devices, body(): value = add_rows(lax.all_gather(value_weight, 'fs', axis=0, tiled=True))  40.8 us
    all_gather x1, waiting for transfers between devices, body(): lax.all_gather(out_weight, 'fs', axis=1, tiled=True)  40.7 us
    all_gather x1, waiting for transfers between devices, body(): bgate = add_rows(lax.all_gather(bgate_weight, 'fs', axis=0, tiled=True))  40 us
  transfers between devices with their start and end apart: 9, of which 9 were waited for; matrix products, arithmetic and copies ran while one was open for 4% of the time, Pallas kernels for 0%

commit v1 on v0

--- a/solution.py
+++ b/solution.py
@@ -5,6 +5,12 @@
 
 LEN = 256
 epsilon = 1e-06
+
+
+def summed_here(array, name):
+    parts = lax.all_gather(array, name, axis=0, tiled=False)
+    total = parts.sum(axis=0)
+    return total
 
 
 def normalize(rows, gain):
@@ -60,7 +66,7 @@
         lax.all_gather(out_weight, "fs", axis=1, tiled=True),
         preferred_element_type=jnp.float32,
     )
-    mixed = lax.psum(partial_mix.astype(jnp.bfloat16), "tp").astype(jnp.float32)
+    mixed = summed_here(partial_mix.astype(jnp.bfloat16), "tp").astype(jnp.float32)
     resid = (whole.astype(jnp.float32) + normalize(mixed, mix_out_gain)).astype(jnp.bfloat16)
     resid_own = lax.dynamic_slice_in_dim(resid, first, own_width, 1)
     second = normalize(resid, ffn_in_gain).astype(jnp.bfloat16)

time: 708 us -> 728 us (1.028)
  other arithmetic: 18.9 us -> 31.7 us
    all_gather x0 -> x1, waiting for transfers between devices: none -> 103 us  [summed_here(): parts = lax.all_gather(array, name, axis=0, tiled=False)]
    psum x1 -> x0, waiting for transfers between devices: 82.7 us -> none  [body(): mixed = lax.psum(partial_mix.astype(jnp.bfloat16), 'tp').astype(jnp.float32)]
    all_gather x1, waiting for transfers between devices: 143 us -> 129 us  [body(): lax.all_gather(up_weight, 'fs', axis=0, tiled=True)]
    reduce_sum x0 -> x1, other arithmetic: none -> 12.3 us  [summed_here(): total = parts.sum(axis=0)]
  transfers between devices with their start and end apart: 9 -> 9, of which waited for: 9 -> 9; matrix products, arithmetic and copies ran while one was open for 4% -> 6% of each run, Pallas kernels for 0% -> 0%
where the time goes in v1:
time: 728 us
  waiting for transfers between devices  629 us (86%)
  matrix products  47.3 us (6%)
  other arithmetic  31.7 us (4%)
  between operations  13.3 us (2%)
    all_gather x1, waiting for transfers between devices, body(): lax.all_gather(down_weight, 'fs', axis=1, tiled=True)  149 us
    all_gather x1, waiting for transfers between devices, body(): lax.all_gather(up_weight, 'fs', axis=0, tiled=True)  129 us
    all_gather x1, waiting for transfers between devices, summed_here(): parts = lax.all_gather(array, name, axis=0, tiled=False)  103 us
    all_gather x1, waiting for transfers between devices, body(): cgate = add_rows(lax.all_gather(cgate_weight, 'fs', axis=0, tiled=True))  44.2 us
    reduce_scatter x1, waiting for transfers between devices, body(): lax.psum_scatter(partial_ffn.astype(jnp.bfloat16), 'tp', scatter_dimensio...  42 us
    all_gather x1, waiting for transfers between devices, body(): value = add_rows(lax.all_gather(value_weight, 'fs', axis=0, tiled=True))  40.8 us
    all_gather x1, waiting for transfers between devices, body(): lax.all_gather(out_weight, 'fs', axis=1, tiled=True)  40.7 us
    all_gather x1, waiting for transfers between devices, body(): bgate = add_rows(lax.all_gather(bgate_weight, 'fs', axis=0, tiled=True))  40 us
  transfers between devices with their start and end apart: 9, of which 9 were waited for; matrix products, arithmetic and copies ran while one was open for 6% of the time, Pallas kernels for 0%

profile of v1, /device:TPU:0, one launch (start us, length us, event | category | flops | bytes accessed | tf_op | source)
XLA Modules:
  0.0 727.9 jit_solution(17972093765376538032)
XLA Ops:
  6.5 0.0 all-gather.10.cloned.1.call-start
  6.5 0.7 all-gather.10.cloned.1.call-update
  7.3 0.0 all-gather.14.cloned.1.call-start
  7.3 0.7 all-gather.14.cloned.1.call-update
  8.0 0.0 all-gather.16.cloned.1.call-start
  8.1 0.7 all-gather.16.cloned.1.call-update
  8.7 0.0 all-gather.12.cloned.1.call-start
  8.8 0.5 all-gather.12.cloned.1.call-update
  9.3 0.0 all-gather.18.cloned.1.call-start
  9.4 0.5 all-gather.18.cloned.1.call-update
  9.9 0.0 all-gather.24.cloned.1.call-start
  10.0 0.7 dynamic-slice_convert_fusion
  10.7 0.7 convert_element_type.78
  11.4 34.8 %all-gather.10.cloned.1.call-done = bf16[1024,2048]{1,0:T(8,128)(2,1)} async-done(((bf16[1024,512]{1,0:T(8,128)(2,1)}), bf16[1024,2048]{1,0:T(8,128)(2,1)}) %all-gather.10.cloned.1.call-update) | async-done | bytes 4194320 | tf_op jit(solution)/shard_map/all_gather | solution.py:48
  46.1 3.1 fusion.5
  49.2 44.2 %all-gather.14.cloned.1.call-done = bf16[2048,512]{1,0:T(8,128)(2,1)} async-done(((bf16[512,512]{1,0:T(8,128)(2,1)}), bf16[2048,512]{1,0:T(8,128)(2,1)}) %all-gather.14.cloned.1.call-update) | async-done | bytes 2097168 | tf_op jit(solution)/shard_map/all_gather | solution.py:55
  93.4 5.2 convolution_convert_fusion.2
  98.6 40.8 %all-gather.16.cloned.1.call-done = bf16[2048,512]{1,0:T(8,128)(2,1)} async-done(((bf16[512,512]{1,0:T(8,128)(2,1)}), bf16[2048,512]{1,0:T(8,128)(2,1)}) %all-gather.16.cloned.1.call-update) | async-done | bytes 2097168 | tf_op jit(solution)/shard_map/all_gather | solution.py:56
  139.4 5.2 convert_multiply_fusion.8
  144.7 0.6 multiply_add_fusion
  145.3 40.0 %all-gather.12.cloned.1.call-done = bf16[2048,512]{1,0:T(8,128)(2,1)} async-done(((bf16[512,512]{1,0:T(8,128)(2,1)}), bf16[2048,512]{1,0:T(8,128)(2,1)}) %all-gather.12.cloned.1.call-update) | async-done | bytes 2097168 | tf_op jit(solution)/shard_map/all_gather | solution.py:54
  185.4 5.2 fusion.25
  190.6 40.7 %all-gather.18.cloned.1.call-done = bf16[512,2048]{1,0:T(8,128)(2,1)} async-done(((bf16[512,512]{1,0:T(8,128)(2,1)}), bf16[512,2048]{1,0:T(8,128)(2,1)}) %all-gather.18.cloned.1.call-update) | async-done | bytes 2097168 | tf_op jit(solution)/shard_map/all_gather | solution.py:66
  231.3 5.9 convolution_convert_fusion
  237.2 0.0 copy-start.1
  237.2 0.0 copy-start.2
  237.2 0.0 all-gather.24.cloned.1.call-update
  237.2 0.0 all-gather.20.cloned.1.call-start
  237.2 0.7 all-gather.20.cloned.1.call-update
  237.9 0.0 all-gather.22.cloned.1.call-start
  238.0 0.7 all-gather.22.cloned.1.call-update
  238.7 0.2 reduce-scatter.2.cloned.1.call-start
  238.9 0.0 copy-done.1
  238.9 0.0 copy-done.2
  239.0 103.1 %all-gather.24.cloned.1.call-done = bf16[4096,2048]{1,0:T(8,128)(2,1)} async-done(((bf16[1024,2048]{1,0:T(8,128)(2,1)}), bf16[4096,2048]{1,0:T(8,128)(2,1)}) %all-gather.24.cloned.1.call-update) | async-done | bytes 16777232 | tf_op jit(solution)/shard_map/all_gather | solution.py:11
  342.0 12.3 %reduce_sum.49 = bf16[1024,2048]{1,0:T(8,128)(2,1)} reduce(bf16[4,1024,2048]{2,1,0:T(8,128)(2,1)} %bitcast.16, bf16[]{:T(256)} %constant.23.clone.1), dimensions={0}, to_apply=%region_1.2 | reduce | flops 6291456 | bytes 20971522 | tf_op jit(solution)/shard_map/reduce_sum | solution.py:12
  354.3 3.6 fusion
  358.0 0.4 copy-done
  358.4 5.4 fusion.2
  363.8 129.4 %all-gather.20.cloned.1.call-done = bf16[2048,2048]{1,0:T(8,128)(2,1)} async-done(((bf16[512,2048]{1,0:T(8,128)(2,1)}), bf16[2048,2048]{1,0:T(8,128)(2,1)}) %all-gather.20.cloned.1.call-update) | async-done | bytes 8388624 | tf_op jit(solution)/shard_map/all_gather | solution.py:75
  493.3 149.4 %all-gather.22.cloned.1.call-done = bf16[2048,2048]{1,0:T(8,128)(2,1)} async-done(((bf16[2048,512]{1,0:T(8,128)(2,1)}), bf16[2048,2048]{1,0:T(8,128)(2,1)}) %all-gather.22.cloned.1.call-update) | async-done | bytes 8388624 | tf_op jit(solution)/shard_map/all_gather | solution.py:81
  642.7 25.7 %fusion.18 = bf16[1024,2048]{1,0:T(8,128)(2,1)} fusion(bf16[2048,2048]{1,0:T(8,128)(2,1)} %all-gather.22.cloned.1.call-done, bf16[2048,2048]{1,0:T(8,128)(2,1)} %all-gather.20.cloned.1.call-done, bf16[1024,2048]{1,0:T(8,128)(2,1)} %get-tuple-element.6, f32[2048]{0:T(1024)S(1)} %convert_element_type.94, f32[1024]{0:T(1024)S(1)} %add_rsqrt_fusion.1), kind=kOutput, calls=%fused_computation.22 | convolution fusion | flops 17196646400 | bytes 25178112 | tf_op jit(solution)/shard_map/dot_general | solution.py:79
  668.3 0.0 reduce-scatter.2.cloned.1.call-update
  668.3 0.8 dynamic-slice_convert_fusion.1
  669.1 42.0 %reduce-scatter.2.cloned.1.call-done = bf16[1024,512]{1,0:T(8,128)(2,1)} async-done(((bf16[1024,2048]{1,0:T(8,128)(2,1)}), bf16[1024,512]{1,0:T(8,128)(2,1)}) %reduce-scatter.2.cloned.1.call-update) | async-done | bytes 1048592 | tf_op jit(solution)/shard_map/reduce_scatter | solution.py:84
  711.1 1.5 fusion.21
  712.6 5.8 psum.7
  718.4 3.0 fusion.24
  (8 shorter events, 0.0 us)
Async XLA Ops:
  6.5 39.6 %all-gather.10.cloned.1.call-start = ((), (), s32[]{:S(2)}) async-start(), calls=%async_computation.1 | async-start | bytes 5242880 | tf_op jit(solution)/shard_map/all_gather | solution.py:48
  7.3 86.1 %all-gather.14.cloned.1.call-start = ((), (), s32[]{:S(2)}) async-start(), calls=%async_computation.3 | async-start | bytes 2621440 | tf_op jit(solution)/shard_map/all_gather | solution.py:55
  8.0 131.4 %all-gather.16.cloned.1.call-start = ((), (), s32[]{:S(2)}) async-start(), calls=%async_computation.4 | async-start | bytes 2621440 | tf_op jit(solution)/shard_map/all_gather | solution.py:56
  8.7 176.6 %all-gather.12.cloned.1.call-start = ((), (), s32[]{:S(2)}) async-start(), calls=%async_computation.2 | async-start | bytes 2621440 | tf_op jit(solution)/shard_map/all_gather | solution.py:54
  9.3 221.9 %all-gather.18.cloned.1.call-start = ((), (), s32[]{:S(2)}) async-start(), calls=%async_computation.5 | async-start | bytes 2621440 | tf_op jit(solution)/shard_map/all_gather | solution.py:66
  9.9 332.1 %all-gather.24.cloned.1.call-start = ((), (), s32[]{:S(2)}) async-start(), calls=%async_computation.9 | async-start | bytes 20971520 | tf_op jit(solution)/shard_map/all_gather | solution.py:11
  237.2 1.8 copy-start.1
  237.2 1.8 copy-start.2
  237.2 256.1 %all-gather.20.cloned.1.call-start = ((), (), s32[]{:S(2)}) async-start(), calls=%async_computation.6 | async-start | bytes 10485760 | tf_op jit(solution)/shard_map/all_gather | solution.py:75
  237.9 404.7 %all-gather.22.cloned.1.call-start = ((), (), s32[]{:S(2)}) async-start(), calls=%async_computation.7 | async-start | bytes 10485760 | tf_op jit(solution)/shard_map/all_gather | solution.py:81
  238.7 472.4 %reduce-scatter.2.cloned.1.call-start = ((), (), s32[]{:S(2)}) async-start(), calls=%async_computation.8 | async-start | bytes 5242880 | tf_op jit(solution)/shard_map/reduce_scatter | solution.py:84
  354.3 4.1 copy-start
Sparse Core Ops, SparseCore 0:
  8.9 37.1 all-gather.9
  47.7 45.6 all-gather.13
  94.9 44.4 all-gather.15
  140.9 44.4 all-gather.11
  186.8 44.4 all-gather.17
  237.3 104.6 all-gather.23
  343.6 149.5 all-gather.19
  494.8 147.7 all-gather.21
  668.5 42.5 reduce-scatter.1
